TPU v7x, 32 devices: a whole 2x2x4 slice. The times are simulated.
32 devices in a mesh: ep: 8 (over z, core), tp: 4 (over y, x).
Axes of the slice: x: 2, y: 2, z: 4, core: 2. Of those that a mesh axis runs over, the one named last changes fastest.
Arguments:
- tokens: bfloat16 [128, 4096], P('ep', 'tp'), may hold values from -40 to 40
- norm_gain: bfloat16 [4096], P('tp'), may hold values from 0.099609375 to 1.8984375
- routes: int32 [128, 4], P('ep'), may hold values from 0 to 7, all different within a row; in each aligned block of 16 rows (0 to 15, 16 to 31, ...) at most 16 rows name the same one
- route_weights: float32 [128, 4], P('ep'), may hold values from 0.05 to 1
- w_gate: bfloat16 [8, 4096, 4096], P('ep', None, 'tp'), may hold values from -0.25 to 0.25
- w_up: bfloat16 [8, 4096, 4096], P('ep', None, 'tp'), may hold values from -0.25 to 0.25
- w_down: bfloat16 [8, 4096, 4096], P('ep', 'tp'), may hold values from -0.0234375 to 0.0234375
Outputs:
- mixed: bfloat16 [128, 4096], P('ep', 'tp')
Inputs may be any that keep to these rules, and one draw needn't show every extreme that they name: `routes`: within the 16 rows of one device, each token names 4 different experts, and no expert is named by more than 16 rows; some expert reaches 16.
All inputs are finite; a program needn't handle non-finite values.
Results may differ from a plain program's by a relative error of at most 0.018.
Values may be sent and summed in bfloat16 or wider, within the bound.
No kernel may reach another device: no remote copies, remote signals or barrier semaphores. Data moves between devices by JAX's collectives and lax.ppermute only.
A program may use at most 64 MiB of HBM per device.

v0:
```python
import jax
import jax.numpy as jnp
from jax import lax
from jax.sharding import PartitionSpec as P


def shards(tokens, norm_gain, routes, route_weights, w_gate, w_up, w_down):
    tok_rows = tokens.shape[0]
    topk = routes.shape[1]
    groups = lax.axis_size("ep")
    capacity = min(tok_rows, max(2, 2 * tok_rows * topk // groups))
    slot_rows = groups * capacity
    flat = routes.reshape(-1)
    order = jnp.arange(flat.shape[0], dtype=jnp.int32)
    earlier = (flat[:, None] == flat[None, :]) & (order[:, None] > order[None, :])
    slot = jnp.sum(earlier.astype(jnp.int32), axis=1)
    target = (flat * capacity + slot).reshape(tok_rows, topk)
    slot_ids = jnp.arange(slot_rows, dtype=jnp.int32)
    picker = jnp.any(target[None, :, :] == slot_ids[:, None, None], axis=2).astype(jnp.bfloat16)
    combine = jnp.sum(
        jnp.where(target[:, :, None] == slot_ids[None, None, :], route_weights[:, :, None], 0.0),
        axis=1,
    )
    whole, gain_whole = (
        lax.all_gather(tokens, "tp", axis=1, tiled=True),
        lax.all_gather(norm_gain.reshape(1, -1), "tp", axis=1, tiled=True),
    )
    full_values = whole.astype(jnp.float32)
    scale = lax.rsqrt(jnp.mean(full_values * full_values, axis=1, keepdims=True) + 1e-05)
    normed = (full_values * scale * gain_whole.astype(jnp.float32)).astype(jnp.bfloat16)
    outbound = jnp.dot(picker, normed, preferred_element_type=jnp.float32).astype(jnp.bfloat16)
    arrived = lax.all_to_all(
        outbound.reshape(groups, capacity, -1), "ep", split_axis=0, concat_axis=0, tiled=True
    ).reshape(slot_rows, -1)
    gate_pre = jnp.dot(arrived, w_gate[0], preferred_element_type=jnp.float32)
    up_pre = jnp.dot(arrived, w_up[0], preferred_element_type=jnp.float32)
    gated = jnp.minimum(gate_pre, 7.0)
    upper = jnp.clip(up_pre, -7.0, 7.0)
    hidden = ((upper + 1.0) * gated * jax.nn.sigmoid(1.702 * gated)).astype(jnp.bfloat16)
    partial_out = jnp.dot(hidden, w_down[0], preferred_element_type=jnp.float32).astype(
        jnp.bfloat16
    )
    summed = (
        lax.psum_scatter(partial_out, "tp", scatter_dimension=1, tiled=True)
        .astype(jnp.float32)
        .astype(jnp.bfloat16)
    )
    returned = lax.all_to_all(
        summed.reshape(groups, capacity, -1), "ep", split_axis=0, concat_axis=0, tiled=True
    ).reshape(slot_rows, -1)
    mixed = jnp.dot(combine, returned.astype(jnp.float32), precision=lax.Precision.HIGHEST)
    return mixed.astype(jnp.bfloat16)


def solution(mesh):
    placed = (
        P("ep", "tp"),
        P("tp"),
        P("ep", None),
        P("ep", None),
        P("ep", None, "tp"),
        P("ep", None, "tp"),
        P("ep", "tp", None),
    )
    return jax.shard_map(
        shards, mesh=mesh, in_specs=placed, out_specs=P("ep", "tp"), check_vma=False
    )
```

profile of v0, /device:TPU:0, one launch (start us, length us, event | category | flops | bytes accessed | tf_op | source)
XLA Modules:
  0.0 120.4 jit_solution(6978321878295605920)
XLA Ops:
  6.5 0.0 reduce-scatter.2.cloned.1.call-start
  6.5 10.1 %all_gather.6 = bf16[16,4096]{1,0:T(8,128)(2,1)S(1)} all-gather(bf16[16,1024]{1,0:T(8,128)(2,1)} %param.7), channel_id=1, replica_groups=mesh['ep'=8,'tp'=4] {'tp'}, dimensions={1}, use_global_device_ids=true | all-gather | bytes 163840 | tf_op jit(solution)/shard_map/all_gather | solution.py:25
  16.7 0.1 fusion.34
  16.8 0.8 copy.21
  17.6 0.1 eq.20
  17.7 0.2 convert_reduce_fusion
  17.9 0.1 reduce_sum.30
  17.9 0.1 copy.22
  18.0 0.7 multiply_add_fusion
  18.7 0.1 fusion.45
  18.8 7.9 %all-gather = bf16[4096]{0:T(1024)(128)(2,1)S(1)} all-gather(bf16[1024]{0:T(1024)(128)(2,1)} %param.8), channel_id=2, replica_groups=mesh['ep'=8,'tp'=4] {'tp'}, dimensions={0}, use_global_device_ids=true | all-gather | bytes 10240 | tf_op jit(solution)/shard_map/all_gather | solution.py:26
  26.7 0.5 convolution_convert_fusion
  27.2 31.2 %all_to_all.10 = bf16[8,16,4096]{2,1,0:T(8,128)(2,1)S(1)} all-to-all(bf16[8,16,4096]{2,1,0:T(8,128)(2,1)S(1)} %bitcast.36), channel_id=1, replica_groups=mesh['ep'=8,'tp'=4] {'ep'}, dimensions={0} | all-to-all | bytes 2097152 | tf_op jit(solution)/shard_map/all_to_all | solution.py:32
  58.4 4.6 %fusion.9 = f32[128,1024]{1,0:T(8,128)S(1)} fusion(bf16[128,4096]{1,0:T(8,128)(2,1)S(1)} %bitcast.34, bf16[1,4096,1024]{2,1,0:T(8,128)(2,1)} %param.11), kind=kOutput, calls=%fused_computation.8 | convolution fusion | flops 1073872896 | bytes 9961472 | tf_op jit(solution)/shard_map/dot_general | solution.py:35
  63.1 0.0 copy-start
  63.1 9.3 %fusion.6 = bf16[128,4096]{1,0:T(8,128)(2,1)} fusion(bf16[1,1024,4096]{2,1,0:T(8,128)(2,1)} %param.13, f32[128,1024]{1,0:T(8,128)S(1)} %fusion.9, bf16[128,4096]{1,0:T(8,128)(2,1)S(1)} %bitcast.35, bf16[1,4096,1024]{2,1,0:T(8,128)(2,1)} %param.12), kind=kOutput, calls=%fused_computation.6 | convolution fusion | flops 2149187584 | bytes 19398656 | tf_op jit(solution)/shard_map/dot_general | solution.py:40
  72.4 0.0 reduce-scatter.2.cloned.1.call-update
  72.4 26.0 %reduce-scatter.2.cloned.1.call-done = bf16[128,1024]{1,0:T(8,128)(2,1)} async-done(((bf16[128,4096]{1,0:T(8,128)(2,1)}), bf16[128,1024]{1,0:T(8,128)(2,1)}) %reduce-scatter.2.cloned.1.call-update) | async-done | bytes 262160 | tf_op jit(solution)/shard_map/reduce_scatter | solution.py:44
  98.4 4.6 %all-to-all-start.1 = ((bf16[8,16,1024]{2,1,0:T(8,128)(2,1)}), bf16[8,16,1024]{2,1,0:T(8,128)(2,1)S(1)}, u32[]{:S(2)}, u32[]{:S(2)}) async-start(bf16[8,16,1024]{2,1,0:T(8,128)(2,1)} %bitcast.38), calls=%async_computation.2 | async-start | bytes 524288 | tf_op jit(solution)/shard_map/all_to_all | solution.py:48
  103.0 0.0 copy-done
  103.1 0.1 select_reduce_fusion
  103.1 9.6 %all-to-all-done.1 = bf16[8,16,1024]{2,1,0:T(8,128)(2,1)S(1)} async-done(((bf16[8,16,1024]{2,1,0:T(8,128)(2,1)}), bf16[8,16,1024]{2,1,0:T(8,128)(2,1)S(1)}, u32[]{:S(2)}, u32[]{:S(2)}) %all-to-all-start.1) | async-done | bytes 262176 | tf_op jit(solution)/shard_map/all_to_all | solution.py:48
  112.8 0.8 convolution_convert_fusion.1
  (2 shorter events, 0.0 us)
Async XLA Ops:
  6.5 91.9 %reduce-scatter.2.cloned.1.call-start = ((), (), s32[]{:S(2)}) async-start(), calls=%async_computation.3 | async-start | bytes 1310720 | tf_op jit(solution)/shard_map/reduce_scatter | solution.py:44
  63.1 40.0 %copy-start = (f32[16,4]{0,1:T(4,128)S(1)}, f32[16,4]{0,1:T(4,128)}, u32[]{:S(2)}) copy-start(f32[16,4]{0,1:T(4,128)} %param.10) | copy-start | bytes 772
  98.4 14.3 %all-to-all-start.1 = ((bf16[8,16,1024]{2,1,0:T(8,128)(2,1)}), bf16[8,16,1024]{2,1,0:T(8,128)(2,1)S(1)}, u32[]{:S(2)}, u32[]{:S(2)}) async-start(bf16[8,16,1024]{2,1,0:T(8,128)(2,1)} %bitcast.38), calls=%async_computation.2 | async-start | bytes 524288 | tf_op jit(solution)/shard_map/all_to_all | solution.py:48
Sparse Core Ops, SparseCore 0:
  72.5 25.8 reduce-scatter.1
where the time goes:
time: 121 us; the launch traced here: 120 us
  blocking collectives  49.2 us (41%)
  waiting for transfers between devices  35.7 us (30%)
  matrix products  15.2 us (13%)
  between operations  13.4 us (11%)
  starting transfers between devices  4.62 us (4%)
    all_to_all x1, blocking collectives, shards(): lax.all_to_all(outbound.reshape(groups, capacity, -1), 'ep', split_axis=0...  31.2 us
    reduce_scatter x1, waiting for transfers between devices, shards(): lax.psum_scatter(partial_out, 'tp', scatter_dimension=1, tiled=True)  26 us
    all_gather x1, blocking collectives, shards(): lax.all_gather(tokens, 'tp', axis=1, tiled=True)  10.1 us
    all_to_all x1, waiting for transfers between devices, shards(): lax.all_to_all(summed.reshape(groups, capacity, -1), 'ep', split_axis=0,...  9.62 us
    dot_general x1, matrix products, shards(): jnp.dot(hidden, w_down[0], preferred_element_type=jnp.float32)  9.29 us
    all_gather x1, blocking collectives, shards(): lax.all_gather(norm_gain.reshape(1, -1), 'tp', axis=1, tiled=True)  7.86 us
    dot_general x1, matrix products, shards(): gate_pre = jnp.dot(arrived, w_gate[0], preferred_element_type=jnp.float32)  4.63 us
    all_to_all x1, starting transfers between devices, shards(): lax.all_to_all(summed.reshape(groups, capacity, -1), 'ep', split_axis=0,...  4.61 us
  transfers between devices with their start and end apart: 2, of which 2 were waited for; matrix products, arithmetic and copies ran while one was open for 0% of the time, Pallas kernels for 0%

commit v1 on v0

--- a/solution.py
+++ b/solution.py
@@ -22,7 +22,7 @@
         axis=1,
     )
     whole, gain_whole = (
-        lax.all_gather(tokens, "tp", axis=1, tiled=True),
+        jnp.concatenate(lax.all_gather(tokens, "tp"), axis=1),
         lax.all_gather(norm_gain.reshape(1, -1), "tp", axis=1, tiled=True),
     )
     full_values = whole.astype(jnp.float32)

time: 121 us -> 121 us (level)
  no operation moved by 1% of the time
where the time goes in v1:
time: 121 us
  blocking collectives  49.2 us (41%)
  waiting for transfers between devices  35.6 us (29%)
  matrix products  15.2 us (13%)
  between operations  13.5 us (11%)
  starting transfers between devices  4.61 us (4%)
  local copies, waits for them, and re-layouts  1.36 us (1%)
  other arithmetic  1.21 us (1%)
    all_to_all x1, blocking collectives, shards(): lax.all_to_all(outbound.reshape(groups, capacity, -1), 'ep', split_axis=0...  31.2 us
    reduce_scatter x1, waiting for transfers between devices, shards(): lax.psum_scatter(partial_out, 'tp', scatter_dimension=1, tiled=True)  26 us
    all_gather x1, blocking collectives, shards(): lax.all_gather(tokens, 'tp')  10.1 us
    all_to_all x1, waiting for transfers between devices, shards(): lax.all_to_all(summed.reshape(groups, capacity, -1), 'ep', split_axis=0,...  9.62 us
    dot_general x1, matrix products, shards(): jnp.dot(hidden, w_down[0], preferred_element_type=jnp.float32)  9.29 us
    all_gather x1, blocking collectives, shards(): lax.all_gather(norm_gain.reshape(1, -1), 'tp', axis=1, tiled=True)  7.86 us
    dot_general x1, matrix products, shards(): gate_pre = jnp.dot(arrived, w_gate[0], preferred_element_type=jnp.float32)  4.63 us
    all_to_all x1, starting transfers between devices, shards(): lax.all_to_all(summed.reshape(groups, capacity, -1), 'ep', split_axis=0,...  4.61 us
  transfers between devices with their start and end apart: 2, of which 2 were waited for; matrix products, arithmetic and copies ran while one was open for 0% of the time, Pallas kernels for 0%

profile of v1, /device:TPU:0, one launch (start us, length us, event | category | flops | bytes accessed | tf_op | source)
XLA Modules:
  0.0 120.8 jit_solution(14975321849657156243)
XLA Ops:
  6.5 0.0 reduce-scatter.2.cloned.1.call-start
  6.5 10.1 %all-gather = bf16[64,1024]{1,0:T(8,128)(2,1)S(1)} all-gather(bf16[16,1024]{1,0:T(8,128)(2,1)} %param.7), channel_id=2, replica_groups=mesh['ep'=8,'tp'=4] {'tp'}, dimensions={0}, use_global_device_ids=true | all-gather | bytes 163840 | tf_op jit(solution)/shard_map/all_gather | solution.py:25
  16.7 0.2 copy.26
  16.9 0.2 copy.27
  17.0 0.1 multiply_reduce_fusion
  17.2 0.8 copy.24
  18.0 0.1 eq.20
  18.0 0.2 convert_reduce_fusion
  18.2 0.1 reduce_sum.30
  18.3 0.1 copy.25
  18.4 0.7 multiply_add_fusion
  19.1 0.1 fusion.41
  19.2 7.9 %all-gather.1 = bf16[4096]{0:T(1024)(128)(2,1)S(1)} all-gather(bf16[1024]{0:T(1024)(128)(2,1)} %param.8), channel_id=3, replica_groups=mesh['ep'=8,'tp'=4] {'tp'}, dimensions={0}, use_global_device_ids=true | all-gather | bytes 10240 | tf_op jit(solution)/shard_map/all_gather | solution.py:26
  27.1 0.5 convolution_convert_fusion
  27.5 31.2 %all_to_all.10 = bf16[8,16,4096]{2,1,0:T(8,128)(2,1)S(1)} all-to-all(bf16[8,16,4096]{2,1,0:T(8,128)(2,1)S(1)} %bitcast.42), channel_id=1, replica_groups=mesh['ep'=8,'tp'=4] {'ep'}, dimensions={0} | all-to-all | bytes 2097152 | tf_op jit(solution)/shard_map/all_to_all | solution.py:32
  58.8 4.6 %fusion.9 = f32[128,1024]{1,0:T(8,128)S(1)} fusion(bf16[128,4096]{1,0:T(8,128)(2,1)S(1)} %bitcast.40, bf16[1,4096,1024]{2,1,0:T(8,128)(2,1)} %param.11), kind=kOutput, calls=%fused_computation.8 | convolution fusion | flops 1073872896 | bytes 9961472 | tf_op jit(solution)/shard_map/dot_general | solution.py:35
  63.4 0.0 copy-start
  63.4 9.3 %fusion.6 = bf16[128,4096]{1,0:T(8,128)(2,1)} fusion(bf16[1,1024,4096]{2,1,0:T(8,128)(2,1)} %param.13, f32[128,1024]{1,0:T(8,128)S(1)} %fusion.9, bf16[128,4096]{1,0:T(8,128)(2,1)S(1)} %bitcast.41, bf16[1,4096,1024]{2,1,0:T(8,128)(2,1)} %param.12), kind=kOutput, calls=%fused_computation.6 | convolution fusion | flops 2149187584 | bytes 19398656 | tf_op jit(solution)/shard_map/dot_general | solution.py:40
  72.7 0.0 reduce-scatter.2.cloned.1.call-update
  72.8 26.0 %reduce-scatter.2.cloned.1.call-done = bf16[128,1024]{1,0:T(8,128)(2,1)} async-done(((bf16[128,4096]{1,0:T(8,128)(2,1)}), bf16[128,1024]{1,0:T(8,128)(2,1)}) %reduce-scatter.2.cloned.1.call-update) | async-done | bytes 262160 | tf_op jit(solution)/shard_map/reduce_scatter | solution.py:44
  98.8 4.6 %all-to-all-start.1 = ((bf16[8,16,1024]{2,1,0:T(8,128)(2,1)}), bf16[8,16,1024]{2,1,0:T(8,128)(2,1)S(1)}, u32[]{:S(2)}, u32[]{:S(2)}) async-start(bf16[8,16,1024]{2,1,0:T(8,128)(2,1)} %bitcast.47), calls=%async_computation.2 | async-start | bytes 524288 | tf_op jit(solution)/shard_map/all_to_all | solution.py:48
  103.4 0.0 copy-done
  103.4 0.1 select_reduce_fusion
  103.5 9.6 %all-to-all-done.1 = bf16[8,16,1024]{2,1,0:T(8,128)(2,1)S(1)} async-done(((bf16[8,16,1024]{2,1,0:T(8,128)(2,1)}), bf16[8,16,1024]{2,1,0:T(8,128)(2,1)S(1)}, u32[]{:S(2)}, u32[]{:S(2)}) %all-to-all-start.1) | async-done | bytes 262176 | tf_op jit(solution)/shard_map/all_to_all | solution.py:48
  113.1 0.8 convolution_convert_fusion.1
  (3 shorter events, 0.0 us)
Async XLA Ops:
  6.5 92.2 %reduce-scatter.2.cloned.1.call-start = ((), (), s32[]{:S(2)}) async-start(), calls=%async_computation.3 | async-start | bytes 1310720 | tf_op jit(solution)/shard_map/reduce_scatter | solution.py:44
  63.4 40.0 %copy-start = (f32[16,4]{0,1:T(4,128)S(1)}, f32[16,4]{0,1:T(4,128)}, u32[]{:S(2)}) copy-start(f32[16,4]{0,1:T(4,128)} %param.10) | copy-start | bytes 772
  98.8 14.3 %all-to-all-start.1 = ((bf16[8,16,1024]{2,1,0:T(8,128)(2,1)}), bf16[8,16,1024]{2,1,0:T(8,128)(2,1)S(1)}, u32[]{:S(2)}, u32[]{:S(2)}) async-start(bf16[8,16,1024]{2,1,0:T(8,128)(2,1)} %bitcast.47), calls=%async_computation.2 | async-start | bytes 524288 | tf_op jit(solution)/shard_map/all_to_all | solution.py:48
Sparse Core Ops, SparseCore 0:
  72.9 25.8 reduce-scatter.1
